TPU v7x, 128 devices: a whole 4x4x4 slice. The times are simulated.
128 devices in a mesh: ep: 128 (over z, y, x, core).
Axes of the slice: x: 4, y: 4, z: 4, core: 2. Of those that a mesh axis runs over, the one named last changes fastest.
Arguments:
- tokens: bfloat16 [8192, 2048], P('ep'), may hold values from -6 to 6
- conv_state: bfloat16 [8192, 3, 1024], P('ep'), may hold values from -6 to 6
- recur_state: float32 [8192, 1024], P('ep'), may hold values from -6 to 6
- w_branch: bfloat16 [2048, 1024], replicated, may hold values from -0.125 to 0.125
- w_gate: bfloat16 [2048, 1024], replicated, may hold values from -0.125 to 0.125
- conv_taps: float32 [4, 1024], replicated, may hold values from -3 to 3
- rate_blocks: bfloat16 [16, 64, 64], replicated, may hold values from -0.75 to 0.75
- input_blocks: bfloat16 [16, 64, 64], replicated, may hold values from -0.75 to 0.75
- decay_param: float32 [1024], replicated, may hold values from 1.5 to 6.5
- w_mix: bfloat16 [1024, 2048], replicated, may hold values from -0.1875 to 0.1875
- gain_pre: float32 [2048], replicated, may hold values from 0.1 to 1.9
- gain_post: float32 [2048], replicated, may hold values from 0.1 to 1.9
- gain_ffn: float32 [2048], replicated, may hold values from 0.1 to 1.9
- gain_out: float32 [2048], replicated, may hold values from 0.1 to 1.9
- routes: int32 [8192, 2], P('ep'), may hold values from 0 to 127, all different within a row; in each aligned block of 64 rows (0 to 63, 64 to 127, ...) at most 3 rows name the same one
- affinity: float32 [8192, 2], P('ep'), may hold values from 0.05 to 1
- w_expert_gate: bfloat16 [128, 2048, 512], P('ep'), may hold values from -0.125 to 0.125
- w_expert_up: bfloat16 [128, 2048, 512], P('ep'), may hold values from -0.125 to 0.125
- w_expert_down: bfloat16 [128, 512, 2048], P('ep'), may hold values from -0.25 to 0.25
Outputs:
- layer_out: bfloat16 [8192, 2048], P('ep')
- conv_next: bfloat16 [8192, 3, 1024], P('ep')
- state_next: float32 [8192, 1024], P('ep')
Inputs may be any that keep to these rules, and one draw needn't show every extreme that they name: `routes`: each row names 2 different experts. Among the 64 rows of one device no expert is named more than 3 times, and in every draw some device names some expert exactly 3 times.
All inputs are finite; a program needn't handle non-finite values.
Results may differ from a plain program's by a relative error of at most 0.014.
Values may be sent and summed in bfloat16 or wider, within the bound.
A program may use at most 128 MiB of HBM per device.

v0:
```python
import functools

import jax
import jax.numpy as jnp
from jax import lax
from jax.experimental import pallas as pl
from jax.experimental.pallas import tpu as pltpu
from jax.sharding import PartitionSpec as P

epsilon = 1e-06
gate_scale = 8.0
planes = 4
chunks = 4


def rms(values, gain):
    return values * lax.rsqrt(jnp.mean(values * values, axis=-1, keepdims=True) + epsilon) * gain


def layer_kernel(
    n, capacity, limit, top,
    tokens, pre, tap, recur, rate_b, input_b, slope, g_pre, g_post, g_ffn, g_out, message,
    wb_hbm, wg_hbm, wm_hbm, eg_hbm, eu_hbm, ed_hbm,
    out, branch_out, state_out,
    wb, wg, wm, normed, gate_act, merged, mix, residual, mall,
    eg, eu, ed, xall, sbuf, rbuf, obuf, cbuf, pbuf, fbuf, total,
    load_sem, ms, mr, zs, zr, ds_, dr, os_, orr, ps, pr,
):
    parts, lots, part = xall.shape
    group = n // planes
    slots = rbuf.shape[1]
    slab = slots // group
    me = lax.axis_index("ep")
    plane, column = me // group, lax.rem(me, group)
    rows, width = tokens.shape
    channels = pre.shape[1]
    block = rate_b.shape[1]
    loads = [
        pltpu.make_async_copy(src, dst, load_sem.at[k])
        for k, (src, dst) in enumerate(
            (
                (wb_hbm, wb), (wg_hbm, wg), (wm_hbm, wm),
                (eg_hbm.at[0], eg), (eu_hbm.at[0], eu), (ed_hbm.at[0], ed),
            )
        )
    ]
    for load in loads:
        load.start()

    barrier = pltpu.get_barrier_semaphore()

    @pl.loop(1, n)
    def _(d):
        pl.semaphore_signal(barrier, inc=1, device_id={"ep": lax.rem(me + d, n)})

    normed[...] = rms(tokens[...].astype(jnp.float32), g_pre[...]).astype(jnp.bfloat16)
    tile = 256
    loads[0].wait()

    @pl.loop(0, channels // tile)
    def _(t):
        cols = pl.ds(pl.multiple_of(t * tile, tile), tile)
        branch_out[:, cols] = jnp.dot(
            normed[...], wb[:, cols], preferred_element_type=jnp.float32
        ).astype(jnp.bfloat16)

    def lanes(k):
        return pl.ds(pl.multiple_of(k * message.shape[1], message.shape[1]), message.shape[1])

    def message_copy(d, landing):
        device = lax.rem(me + d, n)
        spot = device if landing else me
        return pltpu.make_async_remote_copy(
            src_ref=message, dst_ref=mall.at[:, lanes(spot)], send_sem=ms.at[device],
            recv_sem=mr.at[spot], device_id={"ep": device},
            device_id_type=pl.DeviceIdType.MESH,
        )

    pl.semaphore_wait(barrier, n - 1)

    @pl.loop(1, n)
    def _(d):
        message_copy(d, False).start()

    mall[:, lanes(me)] = message[...]
    loads[1].wait()

    @pl.loop(0, channels // tile)
    def _(t):
        cols = pl.ds(pl.multiple_of(t * tile, tile), tile)
        gate_act[:, cols] = jnp.dot(
            normed[...], wg[:, cols], preferred_element_type=jnp.float32
        ).astype(jnp.bfloat16)

    same = lax.broadcasted_iota(jnp.int32, (tile, tile), 0) // block == (
        lax.broadcasted_iota(jnp.int32, (tile, tile), 1) // block
    )

    def spread(ref, t):
        part = ref[pl.ds(t * tile, tile), :].astype(jnp.float32)
        return jnp.where(same, jnp.concatenate([part] * (tile // block), axis=1), 0.0).astype(
            jnp.bfloat16
        )

    for t in range(channels // tile):
        cols = pl.ds(t * tile, tile)
        conv = pre[:, cols] + branch_out[:, cols].astype(jnp.float32) * tap[:, cols]
        conv16 = conv.astype(jnp.bfloat16)
        rate = jax.nn.sigmoid(
            jnp.dot(conv16, spread(rate_b, t), preferred_element_type=jnp.float32)
        )
        inflow = jax.nn.sigmoid(
            jnp.dot(conv16, spread(input_b, t), preferred_element_type=jnp.float32)
        )
        log_decay = rate * slope[:, cols]
        decay = jnp.exp(log_decay)
        rest = -jnp.tanh(log_decay) * (decay * decay + 1.0)
        state = decay * recur[:, cols] + jnp.sqrt(rest) * (inflow * conv)
        state_out[:, cols] = state
        merged[:, cols] = (state * jax.nn.gelu(gate_act[:, cols].astype(jnp.float32))).astype(
            jnp.bfloat16
        )
    loads[2].wait()

    @pl.loop(0, width // tile)
    def _(t):
        cols = pl.ds(pl.multiple_of(t * tile, tile), tile)
        mix[:, cols] = (
            jnp.dot(merged[...], wm[:, cols], preferred_element_type=jnp.float32)
            .astype(jnp.bfloat16)
            .astype(jnp.float32)
        )

    residual[...] = tokens[...].astype(jnp.float32) + rms(mix[...], g_post[...])
    ffn = rms(residual[...], g_ffn[...]).astype(jnp.bfloat16)
    own = pl.ds(pl.multiple_of(plane * rows, rows), rows)
    for c in range(parts):
        xall[c, own] = ffn[:, c * part : (c + 1) * part]

    def along(d):
        other = lax.rem(plane + d, planes)
        return other, other * group + column

    def beside(d):
        other = lax.rem(column + d, group)
        return other, plane * group + other

    def rcopy(src, dst, send, recv, device):
        return pltpu.make_async_remote_copy(
            src_ref=src, dst_ref=dst, send_sem=send, recv_sem=recv,
            device_id={"ep": device}, device_id_type=pl.DeviceIdType.MESH,
        )

    def strip(k):
        return pl.ds(pl.multiple_of(k * slab, slab), slab)

    def seqs(k):
        return pl.ds(pl.multiple_of(k * rows, rows), rows)

    def token_copy(c, d, landing):
        other, device = along(d)
        spot = other if landing else plane
        return rcopy(
            xall.at[c, seqs(plane)], xall.at[c, seqs(spot)], zs.at[c, other],
            zr.at[c, spot], device,
        )

    def slab_copy(c, d, landing, src, dst, send, recv):
        other, device = beside(d)
        spot = other if landing else column
        return rcopy(
            src.at[c, strip(other)], dst.at[c, strip(spot)], send.at[c, other],
            recv.at[c, spot], device,
        )

    def back_copy(c, d, landing):
        other, device = along(d)
        spot = other if landing else plane
        return rcopy(
            pbuf.at[c, seqs(other)], fbuf.at[c, seqs(spot)], ps.at[c, other],
            pr.at[c, spot], device,
        )

    far = list(range(1, planes))
    near = list(range(1, group))
    for c in range(parts):
        for d in far:
            token_copy(c, d, False).start()

    @pl.loop(1, n)
    def _(d):
        message_copy(d, True).wait_recv()

    f32 = jnp.float32
    names = lax.broadcasted_iota(jnp.int32, (group, 1), 0)
    named = (names + plane * group).astype(f32)
    every = jnp.zeros((group, mall.shape[1]), f32)
    for k in range(top):
        every = every + jnp.where(mall[k : k + 1, :] == named, 1.0, 0.0)
    device_at = lax.broadcasted_iota(jnp.int32, every.shape, 1) // message.shape[1]
    lot_at = lax.broadcasted_iota(jnp.int32, (1, lots), 1)
    base = jnp.zeros((group, lots), f32)
    current = []
    for q in range(planes):
        device = q * group + column
        before = jnp.sum(jnp.where(device_at < device, every, 0.0), axis=1, keepdims=True)
        base = jnp.where(lot_at // rows == q, before, base)
        current.append(mall[:, lanes(device)][:, :rows])
    current = jnp.concatenate(current, axis=1)
    one = [jnp.where(current[k : k + 1, :] == named, 1.0, 0.0) for k in range(top)]
    left = lax.broadcasted_iota(jnp.int32, (lots, lots), 0)
    right = lax.broadcasted_iota(jnp.int32, (lots, lots), 1)
    upper = jnp.where((left // rows == right // rows) & (left < right), 1.0, 0.0)
    slot = jnp.dot(
        sum(one).astype(jnp.bfloat16), upper.astype(jnp.bfloat16), preferred_element_type=f32
    )
    spot_of = jnp.where(
        base + slot < limit,
        (names * slab + (lot_at // rows) * capacity + 1).astype(f32) + slot,
        0.0,
    )
    codes = [jnp.sum(one[k] * spot_of, axis=0, keepdims=True) - 1.0 for k in range(top)]
    raw = [current[top + k : top + k + 1, :] for k in range(top)]
    shares = [r / sum(raw) for r in raw]
    spare = [jnp.zeros((1, lots), f32)] * (-2 * top % 8)
    turned = jnp.transpose(jnp.concatenate(codes + shares + spare, axis=0))

    row_at = lax.broadcasted_iota(jnp.int32, (slots, lots), 0).astype(f32)
    pick = jnp.zeros((slots, lots), f32)
    for k in range(top):
        pick = jnp.where(row_at == codes[k], 1.0, pick)
    pick = pick.astype(jnp.bfloat16)
    col_at = lax.broadcasted_iota(jnp.int32, (lots, slots), 1).astype(f32)
    blend = jnp.zeros((lots, slots), f32)
    for k in range(top):
        blend = jnp.where(
            col_at == turned[:, k : k + 1], turned[:, top + k : top + k + 1], blend
        )
    high = blend.astype(jnp.bfloat16)
    low = (blend - high.astype(f32)).astype(jnp.bfloat16)

    sums = [None, None]

    def absorb(c):
        for d in near:
            slab_copy(c, d, True, sbuf, rbuf, ds_, dr).wait_recv()
        got = rbuf[c]
        for k, w in enumerate((eg, eu)):
            piece = jnp.dot(
                got, w[c * part : (c + 1) * part, :], preferred_element_type=jnp.float32
            )
            sums[k] = piece if sums[k] is None else sums[k] + piece

    for c in range(parts):
        for d in far:
            token_copy(c, d, True).wait_recv()
        sbuf[c] = jnp.dot(pick, xall[c], preferred_element_type=jnp.float32).astype(jnp.bfloat16)
        for d in near:
            slab_copy(c, d, False, sbuf, rbuf, ds_, dr).start()
        rbuf[c, strip(column)] = sbuf[c, strip(column)]
        if c == 0:
            for load in loads[3:]:
                load.wait()
        else:
            absorb(c - 1)
    absorb(parts - 1)
    hidden = (jax.nn.silu(sums[0]) * sums[1]).astype(jnp.bfloat16)

    for c in range(parts):
        obuf[c] = jnp.dot(
            hidden, ed[:, c * part : (c + 1) * part], preferred_element_type=jnp.float32
        ).astype(jnp.bfloat16)
        for d in near:
            slab_copy(c, d, False, obuf, cbuf, os_, orr).start()
        cbuf[c, strip(column)] = obuf[c, strip(column)]

    for c in range(parts):
        for d in near:
            slab_copy(c, d, True, obuf, cbuf, os_, orr).wait_recv()
        got = cbuf[c]
        pbuf[c] = (
            jnp.dot(high, got, preferred_element_type=jnp.float32)
            + jnp.dot(low, got, preferred_element_type=jnp.float32)
        ).astype(jnp.bfloat16)
        for d in far:
            back_copy(c, d, False).start()
        fbuf[c, seqs(plane)] = pbuf[c, seqs(plane)]

    squares = jnp.zeros((rows, 1), jnp.float32)
    for c in range(parts):
        for d in far:
            back_copy(c, d, True).wait_recv()
        summed = fbuf[c, 0:rows].astype(jnp.float32)
        for q in range(1, planes):
            summed = summed + fbuf[c, q * rows : (q + 1) * rows].astype(jnp.float32)
        total[c] = summed
        squares = squares + jnp.sum(summed * summed, axis=1, keepdims=True)
    scale = lax.rsqrt(squares / (parts * part) + epsilon)
    for c in range(parts):
        cols = slice(c * part, (c + 1) * part)
        out[:, cols] = (residual[:, cols] + total[c] * scale * g_out[:, cols]).astype(out.dtype)

    @pl.loop(1, n)
    def _(d):
        message_copy(d, False).wait_send()

    for c in range(parts):
        for d in far:
            token_copy(c, d, False).wait_send()
            back_copy(c, d, False).wait_send()
        for d in near:
            slab_copy(c, d, False, sbuf, rbuf, ds_, dr).wait_send()
            slab_copy(c, d, False, obuf, cbuf, os_, orr).wait_send()


def vmem(count):
    return [pl.BlockSpec(memory_space=pltpu.VMEM)] * count


def anywhere(count):
    return [pl.BlockSpec(memory_space=pl.ANY)] * count


def shards(
    tokens, conv_state, recur_state, w_branch, w_gate, conv_taps, rate_blocks, input_blocks,
    decay_param, w_mix, gain_pre, gain_post, gain_ffn, gain_out, routes, affinity,
    w_expert_gate, w_expert_up, w_expert_down,
):
    n = lax.axis_size("ep")
    rows, width = tokens.shape
    channels = recur_state.shape[1]
    top = routes.shape[1]
    hidden = w_expert_gate.shape[2]
    bf16, f32 = jnp.bfloat16, jnp.float32
    group = n // planes
    capacity = max(2, 3 * rows * top // n)
    limit = rows * top // 2
    slab = -(-planes * capacity // 16) * 16
    slots, lots, part = group * slab, planes * rows, width // chunks

    message = jnp.concatenate([routes.T.astype(f32), affinity.T], axis=0)
    message = jnp.pad(
        message, ((0, -2 * top % 8), (0, -rows % 128)), constant_values=-1.0
    )

    row = lambda v: v.reshape(1, -1)
    pre = jnp.sum(conv_state.astype(f32) * conv_taps[None, :-1], axis=1)
    slope = row(-gate_scale * jax.nn.softplus(-decay_param))
    block = rate_blocks.shape[1]
    dma = lambda *count: pltpu.SemaphoreType.DMA(count)
    layer_out, branch, state_next = pl.pallas_call(
        functools.partial(layer_kernel, n, capacity, limit, top),
        out_shape=(
            jax.ShapeDtypeStruct((rows, width), bf16),
            jax.ShapeDtypeStruct((rows, channels), bf16),
            jax.ShapeDtypeStruct((rows, channels), f32),
        ),
        in_specs=vmem(12) + anywhere(6),
        out_specs=tuple(vmem(3)),
        scratch_shapes=[
            pltpu.VMEM((width, channels), bf16),
            pltpu.VMEM((width, channels), bf16),
            pltpu.VMEM((channels, width), bf16),
            pltpu.VMEM((rows, width), bf16),
            pltpu.VMEM((rows, channels), bf16),
            pltpu.VMEM((rows, channels), bf16),
            pltpu.VMEM((rows, width), f32),
            pltpu.VMEM((rows, width), f32),
            pltpu.VMEM((message.shape[0], n * message.shape[1]), f32),
            pltpu.VMEM((width, hidden), bf16),
            pltpu.VMEM((width, hidden), bf16),
            pltpu.VMEM((hidden, width), bf16),
            pltpu.VMEM((chunks, lots, part), bf16),
            pltpu.VMEM((chunks, slots, part), bf16),
            pltpu.VMEM((chunks, slots, part), bf16),
            pltpu.VMEM((chunks, slots, part), bf16),
            pltpu.VMEM((chunks, slots, part), bf16),
            pltpu.VMEM((chunks, lots, part), bf16),
            pltpu.VMEM((chunks, lots, part), bf16),
            pltpu.VMEM((chunks, rows, part), f32),
            dma(6), dma(n), dma(n),
            dma(chunks, planes), dma(chunks, planes), dma(chunks, group), dma(chunks, group),
            dma(chunks, group), dma(chunks, group), dma(chunks, planes), dma(chunks, planes),
        ],
        compiler_params=pltpu.CompilerParams(
            collective_id=0, has_side_effects=True, vmem_limit_bytes=60 << 20
        ),
    )(
        tokens, pre, conv_taps[-1:], recur_state, rate_blocks.reshape(channels, block),
        input_blocks.reshape(channels, block), slope, row(gain_pre), row(gain_post),
        row(gain_ffn), row(gain_out), message,
        w_branch, w_gate, w_mix, w_expert_gate, w_expert_up, w_expert_down,
    )
    conv_next = jnp.concatenate([conv_state[:, 1:], branch[:, None, :]], axis=1)
    return (layer_out, conv_next, state_next)


def solution(mesh):
    ep, copied = "ep", P()
    return jax.shard_map(
        shards,
        mesh=mesh,
        in_specs=(P(ep, None), P(ep, None, None), P(ep, None))
        + (copied,) * 11
        + (P(ep, None),) * 2
        + (P(ep, None, None),) * 3,
        out_specs=(P(ep, None), P(ep, None, None), P(ep, None)),
        check_vma=False,
    )
```

profile of v0, /device:TPU:1, one launch (start us, length us, event | category | flops | bytes accessed | tf_op | source)
XLA Modules:
  0.0 105.0 jit_solution(3988146384114789894)
XLA Ops:
  0.6 0.7 convert_bitcast_fusion
  1.3 1.3 %select_maximum_fusion.message = f32[8,128]{1,0:T(8,128)} fusion(f32[2,64]{1,0:T(2,128)} %bitcast.21, f32[2,64]{1,0:T(2,128)S(1)} %convert_bitcast_fusion), kind=kLoop, calls=%fused_computation.4 | loop fusion | flops 8192 | bytes 5120 | tf_op jit(solution)/shard_map/concatenate | solution.py:341
  2.6 1.3 %fusion = f32[1024]{0:T(1024)} fusion(f32[1024]{0:T(1024)} %param.27), kind=kLoop, calls=%fused_computation.3 | loop fusion | flops 8192 | bytes 8192 | tf_op jit(solution)/shard_map/mul | solution.py:348
  3.9 1.3 %slice.10.tap = f32[1,1024]{1,0:T(1,128)} slice(f32[4,1024]{1,0:T(4,128)} %param.24), slice={[3:4], [0:1024]} | slice | bytes 8192 | tf_op jit(solution)/shard_map/slice | solution.py:389
  5.2 1.8 %multiply_reduce_fusion.pre = f32[64,1024]{1,0:T(8,128)} fusion(bf16[64,3,1024]{2,0,1:T(8,128)(2,1)} %param.20, f32[3,1024]{1,0:T(4,128)} %bitcast.15), kind=kLoop, calls=%fused_computation | loop fusion | flops 524288 | bytes 667648 | tf_op jit(solution)/shard_map/reduce_sum | solution.py:347
  7.0 0.0 slice-start
  7.0 92.9 %shard_map.202 = (bf16[64,2048]{1,0:T(8,128)(2,1)}, bf16[64,1024]{1,0:T(8,128)(2,1)}, f32[64,1024]{1,0:T(8,128)}) custom-call(bf16[64,2048]{1,0:T(8,128)(2,1)} %tokens.1, f32[64,1024]{1,0:T(8,128)} %multiply_reduce_fusion.pre, f32[1,1024]{1,0:T(1,128)} %slice.10.tap, f32[64,1024]{1,0:T(8,128)} %recur.1, bf16[1024,64]{1,0:T(8,128)(2,1)} %bitcast.12, ...), custom_call_target="tpu_custom_call" | custom-call | tf_op jit(solution)/shard_map/pallas_call | solution.py:351
  99.9 0.0 slice-done
  99.9 1.7 %pad_maximum_fusion = bf16[64,3,1024]{2,0,1:T(8,128)(2,1)} fusion(bf16[64,1,1024]{2,0,1:T(8,128)(2,1)} %bitcast.14, bf16[64,2,1024]{2,0,1:T(8,128)(2,1)S(1)} %slice-done), kind=kLoop, calls=%fused_computation.1 | loop fusion | flops 196608 | bytes 786432 | tf_op jit(solution)/shard_map/concatenate | solution.py:394
  101.6 1.7 %copy.24 = bf16[64,2048]{1,0:T(8,128)(2,1)} copy(bf16[64,2048]{1,0:T(8,128)(2,1)} %get-tuple-element.12) | data formatting | bytes 524288
  103.3 1.7 %copy.25 = f32[64,1024]{1,0:T(8,128)} copy(f32[64,1024]{1,0:T(8,128)} %get-tuple-element.14) | data formatting | bytes 524288
Async XLA Ops:
  7.0 92.9 %slice-start = ((bf16[64,3,1024]{2,0,1:T(8,128)(2,1)}), bf16[64,2,1024]{2,0,1:T(8,128)(2,1)S(1)}, s32[]{:S(2)}) async-start(bf16[64,3,1024]{2,0,1:T(8,128)(2,1)} %param.20), calls=%async_computation | async-start | bytes 524288 | tf_op jit(solution)/shard_map/slice | solution.py:394
where the time goes:
time: 105 us
  Pallas kernels  92.9 us (88%)
  other arithmetic  6.75 us (6%)
  local copies, waits for them, and re-layouts  4.66 us (4%)
    pallas_call x1, Pallas kernels, shards(): pl.pallas_call(functools.partial(layer_kernel, n, capacity, limit, top),...  92.9 us
    unnamed x2, local copies, waits for them, and re-layouts  3.34 us

commit v1 on v0

v1 whole, which is shorter than its diff:
```python
import functools

import jax
import jax.numpy as jnp
from jax import lax
from jax.experimental import pallas as pl
from jax.experimental.pallas import tpu as pltpu
from jax.sharding import PartitionSpec as P

epsilon = 1e-06
gate_scale = 8.0
line = 8
lanes = 128
stride = 3
tile = 256
wide = 512


def rms(values, gain):
    return values * lax.rsqrt(jnp.mean(values * values, axis=-1, keepdims=True) + epsilon) * gain


def layer_kernel(
    n, cap, limit, top,
    tokens, conv_state, recur, taps, rate_b, input_b, decay_param,
    g_pre, g_post, g_ffn, g_out, routes, affinity,
    wb_hbm, wg_hbm, wm_hbm, eg_hbm, eu_hbm, ed_hbm,
    out, conv_out, state_out,
    wb, wg, wm, eg, eu, ed, normed, merged, mix, residual, rate_w, input_w,
    stage, rows_x, packed, sbuf, rbuf, obuf, cbuf, otile,
    mrow, mall, tab_v, share_v, etab_v, tab, share, etab,
    load_sem, tab_sem, m_send, m_recv, s_send, s_recv, o_send, o_recv, ready,
):
    f32, bf16 = jnp.float32, jnp.bfloat16
    me = lax.axis_index("ep")
    rows, width = tokens.shape
    channels = recur.shape[1]
    block = rate_b.shape[1]
    parts = width // lanes
    lots = n // line
    outer, inner = me // line, lax.rem(me, line)

    pairs = []
    for t in range(channels // tile):
        cols = pl.ds(t * tile, tile)
        pairs.append((wb_hbm.at[:, cols], wb.at[:, cols]))
        pairs.append((wg_hbm.at[:, cols], wg.at[:, cols]))
    first_mix = len(pairs)
    for t in range(width // wide):
        cols = pl.ds(t * wide, wide)
        pairs.append((wm_hbm.at[:, cols], wm.at[:, cols]))
    first_expert = len(pairs)
    pairs += [(eg_hbm.at[0], eg), (eu_hbm.at[0], eu), (ed_hbm.at[0], ed)]
    loads = [pltpu.make_async_copy(src, dst, load_sem.at[k]) for k, (src, dst) in enumerate(pairs)]
    for load in loads:
        load.start()

    beside = [outer * line + lax.rem(inner + d, line) for d in range(1, line)]
    along = [lax.rem(outer + q, lots) * line + inner for q in range(1, lots)]
    barrier = pltpu.get_barrier_semaphore()
    for device in along + beside:
        pl.semaphore_signal(barrier, inc=1, device_id={"ep": device})

    def rcopy(src, dst, send, recv, device):
        return pltpu.make_async_remote_copy(
            src_ref=src, dst_ref=dst, send_sem=send, recv_sem=recv,
            device_id={"ep": device}, device_id_type=pl.DeviceIdType.MESH,
        )

    flat = top * rows
    row_at = lax.broadcasted_iota(jnp.int32, (flat, flat), 0)
    col_at = lax.broadcasted_iota(jnp.int32, (flat, flat), 1)
    row_s, col_s = lax.rem(row_at, rows), lax.rem(col_at, rows)
    named = jnp.concatenate([routes[k : k + 1, :] for k in range(top)], axis=1)
    mrow[...] = named
    mall[me] = named
    down = jnp.transpose(jnp.broadcast_to(named, (8, flat)))[:, 0:1]
    equal = down == named
    rank_row = jnp.sum(jnp.where(equal & (row_s < col_s), 1, 0), axis=0, keepdims=True)
    rank_col = jnp.sum(jnp.where(equal & (col_s < row_s), 1, 0), axis=1, keepdims=True)
    mine = down == col_at
    table = [
        jnp.sum(jnp.where(mine & (rank_col == r), row_s, 0), axis=0, keepdims=True)
        for r in range(cap)
    ]
    table.append(named * cap + rank_row)
    table += [jnp.zeros((1, flat), jnp.int32)] * (8 - len(table))
    tab_v[...] = jnp.concatenate(table, axis=0)
    amount = affinity[...]
    part = amount / jnp.sum(amount, axis=0, keepdims=True)
    part = jnp.concatenate([part[k : k + 1, :] for k in range(top)], axis=1)
    share_v[...] = jnp.broadcast_to(part, (8, flat))
    to_tab = pltpu.make_async_copy(tab_v, tab, tab_sem.at[0])
    to_share = pltpu.make_async_copy(share_v, share, tab_sem.at[1])
    to_tab.start()
    to_share.start()

    normed[...] = rms(tokens[...].astype(f32), g_pre[...]).astype(bf16)

    same = lax.broadcasted_iota(jnp.int32, (tile, tile), 0) // block == (
        lax.broadcasted_iota(jnp.int32, (tile, tile), 1) // block
    )
    for ref, spread in ((rate_b, rate_w), (input_b, input_w)):
        for t in range(channels // tile):
            piece = ref[pl.ds(t * tile, tile), :].astype(f32)
            spread[t] = jnp.where(
                same, jnp.concatenate([piece] * (tile // block), axis=1), 0.0
            ).astype(bf16)

    softplus = jnp.maximum(-decay_param[...], 0.0) + jnp.log1p(jnp.exp(-jnp.abs(decay_param[...])))
    slope = -gate_scale * softplus
    conv_out[0] = conv_state[1]
    conv_out[1] = conv_state[2]

    pl.semaphore_wait(barrier, len(along) + len(beside))
    for device in beside:
        pl.semaphore_signal(ready, inc=1, device_id={"ep": device})
    for device in beside:
        rcopy(mrow, mall.at[me], m_send.at[0], m_recv.at[0], device).start()

    for t in range(channels // tile):
        cols = slice(t * tile, (t + 1) * tile)
        loads[2 * t].wait()
        branch = jnp.dot(normed[...], wb[:, cols], preferred_element_type=f32).astype(bf16)
        conv_out[2, :, cols] = branch
        conv = branch.astype(f32) * taps[3:4, cols]
        for k in range(3):
            conv = conv + conv_state[k, :, cols].astype(f32) * taps[k : k + 1, cols]
        conv16 = conv.astype(bf16)
        rate = jax.nn.sigmoid(jnp.dot(conv16, rate_w[t], preferred_element_type=f32))
        inflow = jax.nn.sigmoid(jnp.dot(conv16, input_w[t], preferred_element_type=f32))
        log_decay = rate * slope[:, cols]
        decay = jnp.exp(log_decay)
        rest = -jnp.tanh(log_decay) * (decay * decay + 1.0)
        state = decay * recur[:, cols] + jnp.sqrt(rest) * (inflow * conv)
        state_out[:, cols] = state
        loads[2 * t + 1].wait()
        gate = jnp.dot(normed[...], wg[:, cols], preferred_element_type=f32).astype(bf16)
        merged[:, cols] = (state * jax.nn.gelu(gate.astype(f32))).astype(bf16)

    rcopy(mall.at[pl.ds(0, line - 1)], mall.at[pl.ds(0, line - 1)], m_send.at[0], m_recv.at[0], me).wait_recv()
    ours = pl.ds(outer * line, line)
    for device in along:
        rcopy(mall.at[ours], mall.at[ours], m_send.at[1], m_recv.at[1], device).start()

    for t in range(width // wide):
        cols = slice(t * wide, (t + 1) * wide)
        loads[first_mix + t].wait()
        mix[:, cols] = (
            jnp.dot(merged[...], wm[:, cols], preferred_element_type=f32).astype(bf16).astype(f32)
        )
    residual[...] = tokens[...].astype(f32) + rms(mix[...], g_post[...])
    ffn = rms(residual[...], g_ffn[...])
    for j in range(parts):
        stage[pl.ds(j, rows, stride=parts), :] = ffn[:, j * lanes : (j + 1) * lanes]
    rows_x[...] = stage[...].reshape(rows, parts, lanes).astype(bf16)
    to_tab.wait()
    to_share.wait()

    @pl.loop(0, n, unroll=4)
    def _(e):
        for r in range(cap):
            sbuf[e * cap + r] = rows_x[tab[r, e]]

    def block_of(device):
        return pl.ds(device * cap, cap)

    pl.semaphore_wait(ready, len(beside))

    @pl.loop(1, n)
    def _(i):
        device = lax.rem(me + stride * i, n)
        rcopy(sbuf.at[block_of(device)], rbuf.at[block_of(me)], s_send, s_recv, device).start()

    for r in range(cap):
        rbuf[me * cap + r] = sbuf[me * cap + r]

    rcopy(mall.at[pl.ds(0, n - line)], mall.at[pl.ds(0, n - line)], m_send.at[1], m_recv.at[1], me).wait_recv()
    every = mall[...].reshape(n, flat)
    count = jnp.sum(jnp.where(every == me, 1, 0), axis=1, keepdims=True)
    dev_row = lax.broadcasted_iota(jnp.int32, (n, n), 0)
    dev_col = lax.broadcasted_iota(jnp.int32, (n, n), 1)
    base_row = jnp.sum(jnp.where(dev_row < dev_col, count, 0), axis=0, keepdims=True)
    base_col = jnp.sum(jnp.where(dev_row == dev_col, base_row, 0), axis=1, keepdims=True)
    origin = jnp.sum(
        jnp.where(
            (base_col <= dev_col) & (dev_col < base_col + count),
            dev_row * cap + dev_col - base_col, 0,
        ),
        axis=0, keepdims=True,
    )
    table = [origin] + [jnp.minimum(base_row + r, limit) for r in range(cap)]
    table += [jnp.zeros((1, n), jnp.int32)] * (8 - len(table))
    etab_v[...] = jnp.concatenate(table, axis=0)
    to_etab = pltpu.make_async_copy(etab_v, etab, tab_sem.at[2])
    to_etab.start()
    to_etab.wait()
    for load in loads[first_expert:]:
        load.wait()
    otile[limit] = jnp.zeros((parts, lanes), bf16)

    most = pl.ds(0, (n - 1) * cap)
    rcopy(sbuf.at[most], rbuf.at[most], s_send, s_recv, me).wait_recv()

    @pl.loop(0, limit, unroll=4)
    def _(p):
        stage[pl.ds(pl.multiple_of(p * parts, parts), parts), :] = rbuf[etab[0, p]].astype(f32)

    for j in range(parts):
        packed[:, j * lanes : (j + 1) * lanes] = stage[pl.ds(j, limit, stride=parts), :].astype(bf16)
    x = packed[...]
    gate = jnp.dot(x, eg[...], preferred_element_type=f32)
    up = jnp.dot(x, eu[...], preferred_element_type=f32)
    hidden = (jax.nn.silu(gate) * up).astype(bf16)
    for t in range(width // wide):
        result = jnp.dot(hidden, ed[:, t * wide : (t + 1) * wide], preferred_element_type=f32)
        for j in range(wide // lanes):
            stage[pl.ds(t * (wide // lanes) + j, limit, stride=parts), :] = (
                result[:, j * lanes : (j + 1) * lanes]
            )
    otile[pl.ds(0, limit)] = stage[...].reshape(limit, parts, lanes).astype(bf16)

    @pl.loop(0, n, unroll=4)
    def _(d):
        for r in range(cap):
            obuf[d * cap + r] = otile[etab[1 + r, d]]

    @pl.loop(1, n)
    def _(i):
        device = lax.rem(me + stride * i, n)
        rcopy(obuf.at[block_of(device)], cbuf.at[block_of(me)], o_send, o_recv, device).start()

    for r in range(cap):
        cbuf[me * cap + r] = obuf[me * cap + r]

    rcopy(obuf.at[most], cbuf.at[most], o_send, o_recv, me).wait_recv()

    @pl.loop(0, rows, unroll=4)
    def _(s):
        value = jnp.zeros((parts, lanes), f32)
        for k in range(top):
            value = value + share[0, k * rows + s] * cbuf[tab[cap, k * rows + s]].astype(f32)
        stage[pl.ds(pl.multiple_of(s * parts, parts), parts), :] = value

    squares = jnp.zeros((rows, 1), f32)
    for j in range(parts):
        cols = slice(j * lanes, (j + 1) * lanes)
        piece = stage[pl.ds(j, rows, stride=parts), :]
        mix[:, cols] = piece
        squares = squares + jnp.sum(piece * piece, axis=1, keepdims=True)
    scale = lax.rsqrt(squares / width + epsilon)
    out[...] = (residual[...] + mix[...] * scale * g_out[...]).astype(out.dtype)

    head = pl.ds(0, line - 1)
    rest_of = pl.ds(0, (lots - 1) * line)
    rcopy(mall.at[head], mall.at[head], m_send.at[0], m_recv.at[0], me).wait_send()
    rcopy(mall.at[rest_of], mall.at[rest_of], m_send.at[1], m_recv.at[1], me).wait_send()
    rcopy(sbuf.at[most], rbuf.at[most], s_send, s_recv, me).wait_send()
    rcopy(obuf.at[most], cbuf.at[most], o_send, o_recv, me).wait_send()


def finish_kernel(a, b, c, a_out, b_out, c_out, a_buf, b_buf, c_buf, get, put):
    work = ((a, a_buf, a_out), (b, b_buf, b_out), (c, c_buf, c_out))
    ins = [pltpu.make_async_copy(src, buf, get.at[k]) for k, (src, buf, _) in enumerate(work)]
    outs = [pltpu.make_async_copy(buf, dst, put.at[k]) for k, (_, buf, dst) in enumerate(work)]
    for copy in ins:
        copy.start()
    for load, store in zip(ins, outs):
        load.wait()
        store.start()
    for copy in outs:
        copy.wait()


def vmem(count):
    return [pl.BlockSpec(memory_space=pltpu.VMEM)] * count


def hbm(count):
    return [pl.BlockSpec(memory_space=pltpu.HBM)] * count


def shards(
    tokens, conv_state, recur_state, w_branch, w_gate, conv_taps, rate_blocks, input_blocks,
    decay_param, w_mix, gain_pre, gain_post, gain_ffn, gain_out, routes, affinity,
    w_expert_gate, w_expert_up, w_expert_down,
):
    n = lax.axis_size("ep")
    rows, width = tokens.shape
    channels = recur_state.shape[1]
    top = routes.shape[1]
    hidden = w_expert_gate.shape[2]
    bf16, f32, i32 = jnp.bfloat16, jnp.float32, jnp.int32
    cap, limit = 3, 64
    parts = width // lanes
    row = lambda v: v.reshape(1, -1)
    block = rate_blocks.shape[1]
    dma = pltpu.SemaphoreType.DMA
    shapes = (
        jax.ShapeDtypeStruct((rows, width), bf16),
        jax.ShapeDtypeStruct((3, rows, channels), bf16),
        jax.ShapeDtypeStruct((rows, channels), f32),
    )
    exchange = pltpu.VMEM((n * cap, parts, lanes), bf16)
    results = pl.pallas_call(
        functools.partial(layer_kernel, n, cap, limit, top),
        out_shape=shapes,
        in_specs=vmem(13) + hbm(6),
        out_specs=tuple(vmem(3)),
        scratch_shapes=[
            pltpu.VMEM((width, channels), bf16),
            pltpu.VMEM((width, channels), bf16),
            pltpu.VMEM((channels, width), bf16),
            pltpu.VMEM((width, hidden), bf16),
            pltpu.VMEM((width, hidden), bf16),
            pltpu.VMEM((hidden, width), bf16),
            pltpu.VMEM((rows, width), bf16),
            pltpu.VMEM((rows, channels), bf16),
            pltpu.VMEM((rows, width), f32),
            pltpu.VMEM((rows, width), f32),
            pltpu.VMEM((channels // tile, tile, tile), bf16),
            pltpu.VMEM((channels // tile, tile, tile), bf16),
            pltpu.VMEM((rows * parts, lanes), f32),
            pltpu.VMEM((rows, parts, lanes), bf16),
            pltpu.VMEM((limit, width), bf16),
            exchange, exchange, exchange, exchange,
            pltpu.VMEM((limit + 1, parts, lanes), bf16),
            pltpu.VMEM((1, top * rows), i32),
            pltpu.VMEM((n, 1, top * rows), i32),
            pltpu.VMEM((8, top * rows), i32),
            pltpu.VMEM((8, top * rows), f32),
            pltpu.VMEM((8, n), i32),
            pltpu.SMEM((8, top * rows), i32),
            pltpu.SMEM((8, top * rows), f32),
            pltpu.SMEM((8, n), i32),
            dma((2 * channels // tile + width // wide + 3,)),
            dma((3,)), dma((2,)), dma((2,)), dma, dma, dma, dma,
            pltpu.SemaphoreType.REGULAR,
        ],
        compiler_params=pltpu.CompilerParams(
            collective_id=0, has_side_effects=True, vmem_limit_bytes=60 << 20
        ),
    )(
        tokens, conv_state.transpose(1, 0, 2), recur_state, conv_taps,
        rate_blocks.reshape(channels, block), input_blocks.reshape(channels, block),
        row(decay_param), row(gain_pre), row(gain_post), row(gain_ffn), row(gain_out),
        routes.T, affinity.T,
        w_branch, w_gate, w_mix, w_expert_gate, w_expert_up, w_expert_down,
    )
    layer_out, conv_next, state_next = pl.pallas_call(
        finish_kernel,
        out_shape=shapes,
        in_specs=hbm(3),
        out_specs=tuple(hbm(3)),
        scratch_shapes=[pltpu.VMEM(s.shape, s.dtype) for s in shapes] + [dma((3,)), dma((3,))],
    )(*results)
    return (layer_out, conv_next.transpose(1, 0, 2), state_next)


def solution(mesh):
    ep, copied = "ep", P()
    return jax.shard_map(
        shards,
        mesh=mesh,
        in_specs=(P(ep, None), P(ep, None, None), P(ep, None))
        + (copied,) * 11
        + (P(ep, None),) * 2
        + (P(ep, None, None),) * 3,
        out_specs=(P(ep, None), P(ep, None, None), P(ep, None)),
        check_vma=False,
    )
```

time: 105 us -> 63.8 us (0.61)
  Pallas kernels: 92.9 us -> 63 us
  other arithmetic: 6.75 us -> 0 us
  local copies, waits for them, and re-layouts: 4.66 us -> 0 us
    pallas_call x1 -> x2, Pallas kernels: 92.9 us -> 63 us  [the longest x1 61 us: shards(): pl.pallas_call(functools.partial(layer_kernel, n, cap, limit, top), out_s...]
    unnamed x2 -> x0, local copies, waits for them, and re-layouts: 3.34 us -> none
    concatenate x2 -> x0, other arithmetic: 2.97 us -> none  [the longest x1 1.69 us: shards(): conv_next = jnp.concatenate([conv_state[:, 1:], branch[:, None, :]], axis=1)]
    reduce_sum x1 -> x0, other arithmetic: 1.8 us -> none  [shards(): pre = jnp.sum(conv_state.astype(f32) * conv_taps[None, :-1], axis=1)]
    slice x3 -> x0, local copies, waits for them, and re-layouts: 1.32 us -> none  [the longest x1 1.31 us: shards(): conv_taps[-1:]]
    mul x1 -> x0, other arithmetic: 1.3 us -> none  [shards(): slope = row(-gate_scale * jax.nn.softplus(-decay_param))]
where the time goes in v1:
time: 63.8 us; the launch traced here: 63.6 us
  Pallas kernels  63 us (99%)
  between operations  0.65 us (1%)
    pallas_call x1, Pallas kernels, shards(): pl.pallas_call(functools.partial(layer_kernel, n, cap, limit, top), out_s...  61 us
    pallas_call x1, Pallas kernels, shards(): pl.pallas_call(finish_kernel, out_shape=shapes, in_specs=hbm(3), out_spec...  1.96 us

profile of v1, /device:TPU:1, one launch (start us, length us, event | category | flops | bytes accessed | tf_op | source)
XLA Modules:
  0.0 63.6 jit_solution(16725440841245287254)
XLA Ops:
  0.6 61.0 %shard_map.202 = (bf16[64,2048]{1,0:T(8,128)(2,1)}, bf16[3,64,1024]{2,1,0:T(8,128)(2,1)}, f32[64,1024]{1,0:T(8,128)}) custom-call(bf16[64,2048]{1,0:T(8,128)(2,1)} %tokens.1, bf16[3,64,1024]{2,1,0:T(8,128)(2,1)} %bitcast.11, f32[64,1024]{1,0:T(8,128)} %recur.1, f32[4,1024]{1,0:T(4,128)} %taps.1, bf16[1024,64]{1,0:T(8,128)(2,1)} %bitcast.12, ...), custom_call_target="tpu_custom_call" | custom-call | tf_op jit(solution)/shard_map/pallas_call | solution.py:305
  61.6 2.0 %shard_map.203 = (bf16[64,2048]{1,0:T(8,128)(2,1)}, bf16[3,64,1024]{2,1,0:T(8,128)(2,1)}, f32[64,1024]{1,0:T(8,128)}) custom-call(bf16[64,2048]{1,0:T(8,128)(2,1)} %get-tuple-element.9.a, bf16[3,64,1024]{2,1,0:T(8,128)(2,1)} %get-tuple-element.10.b, f32[64,1024]{1,0:T(8,128)} %get-tuple-element.11.c), custom_call_target="tpu_custom_call" | custom-call | tf_op jit(solution)/shard_map/pallas_call | solution.py:350

commit v2 on v1

v2 whole, which is shorter than its diff:
```python
import functools

import jax
import jax.numpy as jnp
from jax import lax
from jax.experimental import pallas as pl
from jax.experimental.pallas import tpu as pltpu
from jax.sharding import PartitionSpec as P

epsilon = 1e-06
gate_scale = 8.0
line = 8
lanes = 128
stride = 3
ahead = 4
tile = 256
wide = 512


def rms(values, gain):
    return values * lax.rsqrt(jnp.mean(values * values, axis=-1, keepdims=True) + epsilon) * gain


def layer_kernel(
    n, cap, limit, top,
    tokens_hbm, conv_hbm, recur_hbm, taps_hbm, rate_hbm, input_hbm, decay_hbm,
    pre_hbm, post_hbm, ffn_hbm, last_hbm, routes_hbm, affinity_hbm,
    wb_hbm, wg_hbm, wm_hbm, eg_hbm, eu_hbm, ed_hbm,
    out_hbm, conv_out_hbm, state_out_hbm,
    tokens, conv_state, recur, taps, rate_b, input_b, decay_param,
    g_pre, g_post, g_ffn, g_out, routes, affinity,
    out, conv_out, state_out,
    wb, wg, wm, eg, eu, ed, normed, branch_b, gate_b, merged, mix, residual, rate_w, input_w,
    stage, rows_x, packed, sbuf, rbuf_a, rbuf_b, obuf, cbuf, otile,
    mrow, mall, tab_v, share_v, etab_v, tab, share, etab,
    load_sem, small_sem, put_sem, tab_sem, m_send, m_recv, s_send, s_recv, o_send, o_recv,
):
    f32, bf16 = jnp.float32, jnp.bfloat16
    me = lax.axis_index("ep")
    rows, width = tokens.shape
    channels = recur.shape[1]
    block = rate_b.shape[1]
    parts = width // lanes
    lots = n // line
    half = n // 2
    turn = pow(stride, -1, n)

    pairs = []
    for t in range(channels // tile):
        cols = pl.ds(t * tile, tile)
        pairs.append((wb_hbm.at[:, cols], wb.at[:, cols]))
        pairs.append((wg_hbm.at[:, cols], wg.at[:, cols]))
    first_mix = len(pairs)
    for t in range(width // wide):
        cols = pl.ds(t * wide, wide)
        pairs.append((wm_hbm.at[:, cols], wm.at[:, cols]))
    first_expert = len(pairs)
    pairs += [(eg_hbm.at[0], eg), (eu_hbm.at[0], eu), (ed_hbm.at[0], ed)]
    loads = [pltpu.make_async_copy(src, dst, load_sem.at[k]) for k, (src, dst) in enumerate(pairs)]
    smalls = [
        pltpu.make_async_copy(src, dst, small_sem.at[k])
        for k, (src, dst) in enumerate(
            (
                (routes_hbm, routes), (affinity_hbm, affinity), (tokens_hbm, tokens),
                (pre_hbm, g_pre), (rate_hbm, rate_b), (input_hbm, input_b), (decay_hbm, decay_param),
                (conv_hbm, conv_state), (taps_hbm, taps), (recur_hbm, recur),
                (post_hbm, g_post), (ffn_hbm, g_ffn), (last_hbm, g_out),
            )
        )
    ]
    for load in smalls + loads[:4]:
        load.start()

    barrier = pltpu.get_barrier_semaphore()

    def greet(i):
        pl.semaphore_signal(barrier, inc=1, device_id={"ep": lax.rem(me + i, n)})

    def each_peer(step):
        @pl.loop(0, lots - 1)
        def _(k):
            for j in range(line):
                step(k * line + j + 1)

        for i in range((lots - 1) * line + 1, n):
            step(i)

    each_peer(greet)
    for load in loads[4:first_mix]:
        load.start()

    def rcopy(src, dst, send, recv, device):
        return pltpu.make_async_remote_copy(
            src_ref=src, dst_ref=dst, send_sem=send, recv_sem=recv,
            device_id={"ep": device}, device_id_type=pl.DeviceIdType.MESH,
        )

    for load in smalls[:2]:
        load.wait()
    flat = top * rows
    row_at = lax.broadcasted_iota(jnp.int32, (flat, flat), 0)
    col_at = lax.broadcasted_iota(jnp.int32, (flat, flat), 1)
    row_s, col_s = lax.rem(row_at, rows), lax.rem(col_at, rows)
    named = jnp.concatenate([routes[k : k + 1, :] for k in range(top)], axis=1)
    mrow[...] = named
    mall[me] = named
    across = lax.rem((named - me + n) * turn, n)
    down = jnp.transpose(jnp.broadcast_to(across, (8, flat)))[:, 0:1]
    equal = down == across
    rank_row = jnp.sum(jnp.where(equal & (row_s < col_s), 1, 0), axis=0, keepdims=True)
    rank_col = jnp.sum(jnp.where(equal & (col_s < row_s), 1, 0), axis=1, keepdims=True)
    mine = down == col_at
    table = [
        jnp.sum(jnp.where(mine & (rank_col == r), row_s, 0), axis=0, keepdims=True)
        for r in range(cap)
    ]
    table.append(across * cap + jnp.minimum(rank_row, cap - 1))
    table += [jnp.zeros((1, flat), jnp.int32)] * (8 - len(table))
    tab_v[...] = jnp.concatenate(table, axis=0)
    amount = affinity[...]
    part = amount / jnp.sum(amount, axis=0, keepdims=True)
    part = jnp.concatenate([part[k : k + 1, :] for k in range(top)], axis=1)
    share_v[...] = jnp.broadcast_to(part, (8, flat))
    to_tab = pltpu.make_async_copy(tab_v, tab, tab_sem.at[0])
    to_share = pltpu.make_async_copy(share_v, share, tab_sem.at[1])
    to_tab.start()
    to_share.start()

    for load in smalls[2:4]:
        load.wait()
    normed[...] = rms(tokens[...].astype(f32), g_pre[...]).astype(bf16)

    for load in loads[first_mix:first_expert]:
        load.start()
    for load in smalls[4:]:
        load.wait()
    same = lax.broadcasted_iota(jnp.int32, (tile, tile), 0) // block == (
        lax.broadcasted_iota(jnp.int32, (tile, tile), 1) // block
    )
    for ref, spread in ((rate_b, rate_w), (input_b, input_w)):
        for t in range(channels // tile):
            piece = ref[pl.ds(t * tile, tile), :].astype(f32)
            spread[t] = jnp.where(
                same, jnp.concatenate([piece] * (tile // block), axis=1), 0.0
            ).astype(bf16)

    softplus = jnp.maximum(-decay_param[...], 0.0) + jnp.log1p(jnp.exp(-jnp.abs(decay_param[...])))
    slope = -gate_scale * softplus
    conv_out[0] = conv_state[1]
    conv_out[1] = conv_state[2]

    steps = channels // tile
    for t in range(steps + 1):
        if t < steps:
            cols = slice(t * tile, (t + 1) * tile)
            loads[2 * t].wait()
            loads[2 * t + 1].wait()
            branch_b[:, cols] = jnp.dot(
                normed[...], wb[:, cols], preferred_element_type=f32
            ).astype(bf16)
            gate_b[:, cols] = jnp.dot(
                normed[...], wg[:, cols], preferred_element_type=f32
            ).astype(bf16)
        if t > 0:
            cols = slice((t - 1) * tile, t * tile)
            branch = branch_b[:, cols]
            conv_out[2, :, cols] = branch
            conv = branch.astype(f32) * taps[3:4, cols]
            for k in range(3):
                conv = conv + conv_state[k, :, cols].astype(f32) * taps[k : k + 1, cols]
            conv16 = conv.astype(bf16)
            rate = jax.nn.sigmoid(jnp.dot(conv16, rate_w[t - 1], preferred_element_type=f32))
            inflow = jax.nn.sigmoid(jnp.dot(conv16, input_w[t - 1], preferred_element_type=f32))
            log_decay = rate * slope[:, cols]
            decay = jnp.exp(log_decay)
            rest = -jnp.tanh(log_decay) * (decay * decay + 1.0)
            state = decay * recur[:, cols] + jnp.sqrt(rest) * (inflow * conv)
            state_out[:, cols] = state
            merged[:, cols] = (state * jax.nn.gelu(gate_b[:, cols].astype(f32))).astype(bf16)

    pl.semaphore_wait(barrier, n - 1)

    def tell(i):
        rcopy(mrow, mall.at[me], m_send, m_recv, lax.rem(me + stride * i, n)).start()

    each_peer(tell)

    for t in range(width // wide):
        cols = slice(t * wide, (t + 1) * wide)
        loads[first_mix + t].wait()
        mix[:, cols] = (
            jnp.dot(merged[...], wm[:, cols], preferred_element_type=f32).astype(bf16).astype(f32)
        )
    for load in loads[first_expert:]:
        load.start()
    residual[...] = tokens[...].astype(f32) + rms(mix[...], g_post[...])
    ffn = rms(residual[...], g_ffn[...])
    for j in range(parts):
        stage[pl.ds(j, rows, stride=parts), :] = ffn[:, j * lanes : (j + 1) * lanes]
    rows_x[...] = stage[...].reshape(rows, parts, lanes).astype(bf16)
    to_tab.wait()
    to_share.wait()

    def block_of(i):
        return pl.ds(i * cap, cap)

    def fetch(i):
        for r in range(cap):
            sbuf[i * cap + r] = rows_x[tab[r, i]]

    def send(i, landing, origin, k):
        rcopy(
            sbuf.at[block_of(i)], landing.at[block_of(i - origin)], s_send.at[k], s_recv.at[k],
            lax.rem(me + stride * i, n),
        ).start()

    for i in range(ahead + 1):
        fetch(i)

    @pl.loop(1, half)
    def _(i):
        fetch(i + ahead)
        send(i, rbuf_a, 0, 0)

    @pl.loop(half, n - ahead)
    def _(i):
        fetch(i + ahead)
        send(i, rbuf_b, half, 1)

    for i in range(n - ahead, n):
        send(i, rbuf_b, half, 1)

    put_conv = pltpu.make_async_copy(conv_out, conv_out_hbm, put_sem.at[0])
    put_state = pltpu.make_async_copy(state_out, state_out_hbm, put_sem.at[1])
    put_conv.start()
    put_state.start()
    rbuf_a[block_of(0)] = sbuf[block_of(0)]

    others = pl.ds(0, n - 1)
    rcopy(mall.at[others], mall.at[others], m_send, m_recv, me).wait_recv()
    every = mall[...].reshape(n, flat)
    count = jnp.minimum(jnp.sum(jnp.where(every == me, 1, 0), axis=1, keepdims=True), cap)
    dev_row = lax.broadcasted_iota(jnp.int32, (n, n), 0)
    dev_col = lax.broadcasted_iota(jnp.int32, (n, n), 1)
    eye = dev_row == dev_col
    earlier = dev_row < dev_col

    def turned(column):
        return jnp.sum(jnp.where(eye, column, 0), axis=0, keepdims=True)

    def upright(line_of):
        return jnp.sum(jnp.where(eye, line_of, 0), axis=1, keepdims=True)

    def before(column):
        return jnp.sum(jnp.where(earlier, column, 0), axis=0, keepdims=True)

    kept = jnp.clip(limit - upright(before(count)), 0, count)
    slot = lax.rem((me - dev_row[:, 0:1] + n) * turn, n)
    soon = slot < half
    place = jnp.where(
        lax.rem((me - dev_col[0:1, :] + n) * turn, n) < half,
        before(jnp.where(soon, kept, 0)), before(jnp.where(soon, 0, kept)),
    )
    place_col = upright(place)
    inside = (place_col <= dev_col) & (dev_col < place_col + kept)
    origin = slot * cap + dev_col - place_col
    table = [
        jnp.sum(jnp.where(inside & soon, origin, 0), axis=0, keepdims=True),
        jnp.sum(jnp.where(inside & (slot >= half), origin - half * cap, 0), axis=0, keepdims=True),
    ]
    kept_row = turned(kept)
    table += [jnp.where(kept_row > r, place + r, limit) for r in range(cap)]
    table += [jnp.zeros((1, n), jnp.int32)] * (8 - len(table))
    etab_v[...] = jnp.concatenate(table, axis=0)
    to_etab = pltpu.make_async_copy(etab_v, etab, tab_sem.at[2])
    to_etab.start()
    to_etab.wait()
    for load in loads[first_expert:]:
        load.wait()
    otile[limit] = jnp.zeros((parts, lanes), bf16)

    def fetch_back(i):
        device = lax.rem(me - stride * i + stride * n, n)
        for r in range(cap):
            obuf[i * cap + r] = otile[etab[2 + r, device]]

    def send_back(i, k):
        rcopy(
            obuf.at[block_of(i)], cbuf.at[block_of(i)], o_send.at[k], o_recv.at[k],
            lax.rem(me - stride * i + stride * n, n),
        ).start()

    def expert(landing, k):
        @pl.loop(0, limit, unroll=4)
        def _(p):
            stage[pl.ds(pl.multiple_of(p * parts, parts), parts), :] = (
                landing[etab[k, p]].astype(f32)
            )

        for j in range(parts):
            packed[:, j * lanes : (j + 1) * lanes] = (
                stage[pl.ds(j, limit, stride=parts), :].astype(bf16)
            )
        x = packed[...]
        gate = jnp.dot(x, eg[...], preferred_element_type=f32)
        up = jnp.dot(x, eu[...], preferred_element_type=f32)
        hidden = (jax.nn.silu(gate) * up).astype(bf16)
        for t in range(width // wide):
            result = jnp.dot(hidden, ed[:, t * wide : (t + 1) * wide], preferred_element_type=f32)
            for j in range(wide // lanes):
                stage[pl.ds(t * (wide // lanes) + j, limit, stride=parts), :] = (
                    result[:, j * lanes : (j + 1) * lanes]
                )
        otile[pl.ds(0, limit)] = stage[...].reshape(limit, parts, lanes).astype(bf16)

    def wait_rows(landing, count_of, k):
        some = pl.ds(0, count_of * cap)
        rcopy(sbuf.at[some], landing.at[some], s_send.at[k], s_recv.at[k], me).wait_recv()

    wait_rows(rbuf_a, half - 1, 0)
    expert(rbuf_a, 0)
    for i in range(ahead + 1):
        fetch_back(i)

    @pl.loop(1, half - ahead)
    def _(i):
        fetch_back(i + ahead)
        send_back(i, 0)

    for i in range(half - ahead, half):
        send_back(i, 0)
    cbuf[block_of(0)] = obuf[block_of(0)]

    wait_rows(rbuf_b, n - half, 1)
    expert(rbuf_b, 1)
    for i in range(half, half + ahead):
        fetch_back(i)

    @pl.loop(half, n - ahead)
    def _(i):
        fetch_back(i + ahead)
        send_back(i, 1)

    for i in range(n - ahead, n):
        send_back(i, 1)

    low, high = pl.ds(0, (half - 1) * cap), pl.ds(0, (n - half) * cap)
    rcopy(obuf.at[low], cbuf.at[low], o_send.at[0], o_recv.at[0], me).wait_recv()
    rcopy(obuf.at[high], cbuf.at[high], o_send.at[1], o_recv.at[1], me).wait_recv()

    @pl.loop(0, rows, unroll=4)
    def _(s):
        value = jnp.zeros((parts, lanes), f32)
        for k in range(top):
            value = value + share[0, k * rows + s] * cbuf[tab[cap, k * rows + s]].astype(f32)
        stage[pl.ds(pl.multiple_of(s * parts, parts), parts), :] = value

    squares = jnp.zeros((rows, 1), f32)
    for j in range(parts):
        cols = slice(j * lanes, (j + 1) * lanes)
        piece = stage[pl.ds(j, rows, stride=parts), :]
        mix[:, cols] = piece
        squares = squares + jnp.sum(piece * piece, axis=1, keepdims=True)
    scale = lax.rsqrt(squares / width + epsilon)
    out[...] = (residual[...] + mix[...] * scale * g_out[...]).astype(out.dtype)
    put_out = pltpu.make_async_copy(out, out_hbm, put_sem.at[2])
    put_out.start()

    rcopy(mall.at[others], mall.at[others], m_send, m_recv, me).wait_send()
    for k, some in enumerate((low, high)):
        rcopy(sbuf.at[some], cbuf.at[some], s_send.at[k], s_recv.at[k], me).wait_send()
        rcopy(obuf.at[some], cbuf.at[some], o_send.at[k], o_recv.at[k], me).wait_send()
    put_conv.wait()
    put_state.wait()
    put_out.wait()


def finish_kernel(a, b, c, a_out, b_out, c_out, a_buf, b_buf, c_buf, get, put):
    work = ((a, a_buf, a_out), (b, b_buf, b_out), (c, c_buf, c_out))
    ins = [pltpu.make_async_copy(src, buf, get.at[k]) for k, (src, buf, _) in enumerate(work)]
    outs = [pltpu.make_async_copy(buf, dst, put.at[k]) for k, (_, buf, dst) in enumerate(work)]
    for copy in ins:
        copy.start()
    for load, store in zip(ins, outs):
        load.wait()
        store.start()
    for copy in outs:
        copy.wait()


def hbm(count):
    return [pl.BlockSpec(memory_space=pltpu.HBM)] * count


def shards(
    tokens, conv_state, recur_state, w_branch, w_gate, conv_taps, rate_blocks, input_blocks,
    decay_param, w_mix, gain_pre, gain_post, gain_ffn, gain_out, routes, affinity,
    w_expert_gate, w_expert_up, w_expert_down,
):
    n = lax.axis_size("ep")
    rows, width = tokens.shape
    channels = recur_state.shape[1]
    top = routes.shape[1]
    hidden = w_expert_gate.shape[2]
    bf16, f32, i32 = jnp.bfloat16, jnp.float32, jnp.int32
    cap, limit = 3, 64
    parts = width // lanes
    row = lambda v: v.reshape(1, -1)
    block = rate_blocks.shape[1]
    dma = pltpu.SemaphoreType.DMA
    shapes = (
        jax.ShapeDtypeStruct((rows, width), bf16),
        jax.ShapeDtypeStruct((3, rows, channels), bf16),
        jax.ShapeDtypeStruct((rows, channels), f32),
    )
    small = (
        tokens, conv_state.transpose(1, 0, 2), recur_state, conv_taps,
        rate_blocks.reshape(channels, block), input_blocks.reshape(channels, block),
        row(decay_param), row(gain_pre), row(gain_post), row(gain_ffn), row(gain_out),
        routes.T, affinity.T,
    )
    half = n // 2
    exchange = pltpu.VMEM((n * cap, parts, lanes), bf16)
    exchange_a = pltpu.VMEM((half * cap, parts, lanes), bf16)
    exchange_b = pltpu.VMEM(((n - half) * cap, parts, lanes), bf16)
    results = pl.pallas_call(
        functools.partial(layer_kernel, n, cap, limit, top),
        out_shape=shapes,
        in_specs=hbm(19),
        out_specs=tuple(hbm(3)),
        scratch_shapes=[pltpu.VMEM(v.shape, v.dtype) for v in small + shapes]
        + [
            pltpu.VMEM((width, channels), bf16),
            pltpu.VMEM((width, channels), bf16),
            pltpu.VMEM((channels, width), bf16),
            pltpu.VMEM((width, hidden), bf16),
            pltpu.VMEM((width, hidden), bf16),
            pltpu.VMEM((hidden, width), bf16),
            pltpu.VMEM((rows, width), bf16),
            pltpu.VMEM((rows, channels), bf16),
            pltpu.VMEM((rows, channels), bf16),
            pltpu.VMEM((rows, channels), bf16),
            pltpu.VMEM((rows, width), f32),
            pltpu.VMEM((rows, width), f32),
            pltpu.VMEM((channels // tile, tile, tile), bf16),
            pltpu.VMEM((channels // tile, tile, tile), bf16),
            pltpu.VMEM((rows * parts, lanes), f32),
            pltpu.VMEM((rows, parts, lanes), bf16),
            pltpu.VMEM((limit, width), bf16),
            exchange, exchange_a, exchange_b, exchange, exchange,
            pltpu.VMEM((limit + 1, parts, lanes), bf16),
            pltpu.VMEM((1, top * rows), i32),
            pltpu.VMEM((n, 1, top * rows), i32),
            pltpu.VMEM((8, top * rows), i32),
            pltpu.VMEM((8, top * rows), f32),
            pltpu.VMEM((8, n), i32),
            pltpu.SMEM((8, top * rows), i32),
            pltpu.SMEM((8, top * rows), f32),
            pltpu.SMEM((8, n), i32),
            dma((2 * channels // tile + width // wide + 3,)),
            dma((len(small),)), dma((3,)), dma((3,)), dma, dma, dma((2,)), dma((2,)), dma((2,)), dma((2,)),
        ],
        compiler_params=pltpu.CompilerParams(
            collective_id=0, has_side_effects=True, vmem_limit_bytes=60 << 20
        ),
    )(
        *small, w_branch, w_gate, w_mix, w_expert_gate, w_expert_up, w_expert_down,
    )
    layer_out, conv_next, state_next = pl.pallas_call(
        finish_kernel,
        out_shape=shapes,
        in_specs=hbm(3),
        out_specs=tuple(hbm(3)),
        scratch_shapes=[pltpu.VMEM(s.shape, s.dtype) for s in shapes] + [dma((3,)), dma((3,))],
    )(*results)
    return (layer_out, conv_next.transpose(1, 0, 2), state_next)


def solution(mesh):
    ep, copied = "ep", P()
    return jax.shard_map(
        shards,
        mesh=mesh,
        in_specs=(P(ep, None), P(ep, None, None), P(ep, None))
        + (copied,) * 11
        + (P(ep, None),) * 2
        + (P(ep, None, None),) * 3,
        out_specs=(P(ep, None), P(ep, None, None), P(ep, None)),
        check_vma=False,
    )
```

time: 63.8 us -> 56.3 us (0.88)
  Pallas kernels: 63 us -> 55.5 us
    pallas_call x1, Pallas kernels: 61 us -> 53.5 us  [shards(): pl.pallas_call(functools.partial(layer_kernel, n, cap, limit, top), out_s...]
where the time goes in v2:
time: 56.3 us; the launch traced here: 56.1 us
  Pallas kernels  55.5 us (99%)
  between operations  0.65 us (1%)
    pallas_call x1, Pallas kernels, shards(): pl.pallas_call(functools.partial(layer_kernel, n, cap, limit, top), out_s...  53.5 us
    pallas_call x1, Pallas kernels, shards(): pl.pallas_call(finish_kernel, out_shape=shapes, in_specs=hbm(3), out_spec...  1.96 us

profile of v2, /device:TPU:1, one launch (start us, length us, event | category | flops | bytes accessed | tf_op | source)
XLA Modules:
  0.0 56.1 jit_solution(17693130295294234935)
XLA Ops:
  0.6 53.5 %shard_map.202 = (bf16[64,2048]{1,0:T(8,128)(2,1)}, bf16[3,64,1024]{2,1,0:T(8,128)(2,1)}, f32[64,1024]{1,0:T(8,128)}) custom-call(bf16[64,2048]{1,0:T(8,128)(2,1)} %tokens_hbm.1, bf16[3,64,1024]{2,1,0:T(8,128)(2,1)} %bitcast.11, f32[64,1024]{1,0:T(8,128)} %recur_hbm.1, f32[4,1024]{1,0:T(4,128)} %taps_hbm.1, bf16[1024,64]{1,0:T(8,128)(2,1)} %bitcast.12, ...), custom_call_target="tpu_custom_call" | custom-call | tf_op jit(solution)/shard_map/pallas_call | solution.py:426
  54.2 2.0 %shard_map.203 = (bf16[64,2048]{1,0:T(8,128)(2,1)}, bf16[3,64,1024]{2,1,0:T(8,128)(2,1)}, f32[64,1024]{1,0:T(8,128)}) custom-call(bf16[64,2048]{1,0:T(8,128)(2,1)} %get-tuple-element.9.a, bf16[3,64,1024]{2,1,0:T(8,128)(2,1)} %get-tuple-element.10.b, f32[64,1024]{1,0:T(8,128)} %get-tuple-element.11.c), custom_call_target="tpu_custom_call" | custom-call | tf_op jit(solution)/shard_map/pallas_call | solution.py:469

commit v3 on v2

--- a/solution.py
+++ b/solution.py
@@ -11,7 +11,7 @@
 gate_scale = 8.0
 line = 8
 lanes = 128
-stride = 3
+stride = 21
 ahead = 4
 tile = 256
 wide = 512
@@ -68,7 +68,7 @@
             )
         )
     ]
-    for load in smalls + loads[:4]:
+    for load in smalls[:4] + loads[:2]:
         load.start()
 
     barrier = pltpu.get_barrier_semaphore()
@@ -76,16 +76,21 @@
     def greet(i):
         pl.semaphore_signal(barrier, inc=1, device_id={"ep": lax.rem(me + i, n)})
 
-    def each_peer(step):
-        @pl.loop(0, lots - 1)
+    def peers(step, begin, end):
+        count = (end - begin) // line
+
+        @pl.loop(0, count)
         def _(k):
             for j in range(line):
-                step(k * line + j + 1)
-
-        for i in range((lots - 1) * line + 1, n):
+                step(begin + k * line + j)
+
+        for i in range(begin + count * line, end):
             step(i)
 
-    each_peer(greet)
+    peers(greet, 1, n // 2)
+    for load in smalls[4:] + loads[2:4]:
+        load.start()
+    peers(greet, n // 2, n)
     for load in loads[4:first_mix]:
         load.start()
 
@@ -132,35 +137,37 @@
 
     for load in loads[first_mix:first_expert]:
         load.start()
-    for load in smalls[4:]:
-        load.wait()
-    same = lax.broadcasted_iota(jnp.int32, (tile, tile), 0) // block == (
-        lax.broadcasted_iota(jnp.int32, (tile, tile), 1) // block
-    )
-    for ref, spread in ((rate_b, rate_w), (input_b, input_w)):
-        for t in range(channels // tile):
-            piece = ref[pl.ds(t * tile, tile), :].astype(f32)
-            spread[t] = jnp.where(
-                same, jnp.concatenate([piece] * (tile // block), axis=1), 0.0
-            ).astype(bf16)
-
-    softplus = jnp.maximum(-decay_param[...], 0.0) + jnp.log1p(jnp.exp(-jnp.abs(decay_param[...])))
-    slope = -gate_scale * softplus
-    conv_out[0] = conv_state[1]
-    conv_out[1] = conv_state[2]
-
     steps = channels // tile
     for t in range(steps + 1):
         if t < steps:
             cols = slice(t * tile, (t + 1) * tile)
             loads[2 * t].wait()
             loads[2 * t + 1].wait()
+            if t == 1:
+                for load in smalls[4:]:
+                    load.wait()
             branch_b[:, cols] = jnp.dot(
                 normed[...], wb[:, cols], preferred_element_type=f32
             ).astype(bf16)
             gate_b[:, cols] = jnp.dot(
                 normed[...], wg[:, cols], preferred_element_type=f32
             ).astype(bf16)
+        if t == 1:
+            same = lax.broadcasted_iota(jnp.int32, (tile, tile), 0) // block == (
+                lax.broadcasted_iota(jnp.int32, (tile, tile), 1) // block
+            )
+            for ref, spread in ((rate_b, rate_w), (input_b, input_w)):
+                for u in range(steps):
+                    piece = ref[pl.ds(u * tile, tile), :].astype(f32)
+                    spread[u] = jnp.where(
+                        same, jnp.concatenate([piece] * (tile // block), axis=1), 0.0
+                    ).astype(bf16)
+
+            softplus = jnp.maximum(-decay_param[...], 0.0) + jnp.log1p(jnp.exp(-jnp.abs(decay_param[...])))
+            slope = -gate_scale * softplus
+            conv_out[0] = conv_state[1]
+            conv_out[1] = conv_state[2]
+
         if t > 0:
             cols = slice((t - 1) * tile, t * tile)
             branch = branch_b[:, cols]
@@ -183,11 +190,12 @@
     def tell(i):
         rcopy(mrow, mall.at[me], m_send, m_recv, lax.rem(me + stride * i, n)).start()
 
-    each_peer(tell)
-
+    peers(tell, 1, n)
+
+    for load in loads[first_mix:first_expert]:
+        load.wait()
     for t in range(width // wide):
         cols = slice(t * wide, (t + 1) * wide)
-        loads[first_mix + t].wait()
         mix[:, cols] = (
             jnp.dot(merged[...], wm[:, cols], preferred_element_type=f32).astype(bf16).astype(f32)
         )

time: 56.3 us -> 54.8 us (0.973)
  Pallas kernels: 55.5 us -> 54 us
    pallas_call x1, Pallas kernels: 53.5 us -> 52 us  [shards(): pl.pallas_call(functools.partial(layer_kernel, n, cap, limit, top), out_s...]
where the time goes in v3:
time: 54.8 us; the launch traced here: 54.6 us
  Pallas kernels  54 us (99%)
  between operations  0.65 us (1%)
    pallas_call x1, Pallas kernels, shards(): pl.pallas_call(functools.partial(layer_kernel, n, cap, limit, top), out_s...  52 us
    pallas_call x1, Pallas kernels, shards(): pl.pallas_call(finish_kernel, out_shape=shapes, in_specs=hbm(3), out_spec...  1.96 us

profile of v3, /device:TPU:1, one launch (start us, length us, event | category | flops | bytes accessed | tf_op | source)
XLA Modules:
  0.0 54.6 jit_solution(16875992408554984760)
XLA Ops:
  0.6 52.0 %shard_map.202 = (bf16[64,2048]{1,0:T(8,128)(2,1)}, bf16[3,64,1024]{2,1,0:T(8,128)(2,1)}, f32[64,1024]{1,0:T(8,128)}) custom-call(bf16[64,2048]{1,0:T(8,128)(2,1)} %tokens_hbm.1, bf16[3,64,1024]{2,1,0:T(8,128)(2,1)} %bitcast.11, f32[64,1024]{1,0:T(8,128)} %recur_hbm.1, f32[4,1024]{1,0:T(4,128)} %taps_hbm.1, bf16[1024,64]{1,0:T(8,128)(2,1)} %bitcast.12, ...), custom_call_target="tpu_custom_call" | custom-call | tf_op jit(solution)/shard_map/pallas_call | solution.py:434
  52.7 2.0 %shard_map.203 = (bf16[64,2048]{1,0:T(8,128)(2,1)}, bf16[3,64,1024]{2,1,0:T(8,128)(2,1)}, f32[64,1024]{1,0:T(8,128)}) custom-call(bf16[64,2048]{1,0:T(8,128)(2,1)} %get-tuple-element.9.a, bf16[3,64,1024]{2,1,0:T(8,128)(2,1)} %get-tuple-element.10.b, f32[64,1024]{1,0:T(8,128)} %get-tuple-element.11.c), custom_call_target="tpu_custom_call" | custom-call | tf_op jit(solution)/shard_map/pallas_call | solution.py:477

commit v4 on v3

--- a/solution.py
+++ b/solution.py
@@ -299,7 +299,7 @@
         ).start()
 
     def expert(landing, k):
-        @pl.loop(0, limit, unroll=4)
+        @pl.loop(0, limit, unroll=8)
         def _(p):
             stage[pl.ds(pl.multiple_of(p * parts, parts), parts), :] = (
                 landing[etab[k, p]].astype(f32)
@@ -356,7 +356,7 @@
     rcopy(obuf.at[low], cbuf.at[low], o_send.at[0], o_recv.at[0], me).wait_recv()
     rcopy(obuf.at[high], cbuf.at[high], o_send.at[1], o_recv.at[1], me).wait_recv()
 
-    @pl.loop(0, rows, unroll=4)
+    @pl.loop(0, rows, unroll=8)
     def _(s):
         value = jnp.zeros((parts, lanes), f32)
         for k in range(top):

time: 54.8 us -> 54.7 us (level)
  no operation moved by 1% of the time
where the time goes in v4:
time: 54.7 us; the launch traced here: 54.6 us
  Pallas kernels  53.9 us (99%)
  between operations  0.65 us (1%)
    pallas_call x1, Pallas kernels, shards(): pl.pallas_call(functools.partial(layer_kernel, n, cap, limit, top), out_s...  51.9 us
    pallas_call x1, Pallas kernels, shards(): pl.pallas_call(finish_kernel, out_shape=shapes, in_specs=hbm(3), out_spec...  1.96 us

profile of v4, /device:TPU:1, one launch (start us, length us, event | category | flops | bytes accessed | tf_op | source)
XLA Modules:
  0.0 54.6 jit_solution(8291207558403694877)
XLA Ops:
  0.6 51.9 %shard_map.202 = (bf16[64,2048]{1,0:T(8,128)(2,1)}, bf16[3,64,1024]{2,1,0:T(8,128)(2,1)}, f32[64,1024]{1,0:T(8,128)}) custom-call(bf16[64,2048]{1,0:T(8,128)(2,1)} %tokens_hbm.1, bf16[3,64,1024]{2,1,0:T(8,128)(2,1)} %bitcast.11, f32[64,1024]{1,0:T(8,128)} %recur_hbm.1, f32[4,1024]{1,0:T(4,128)} %taps_hbm.1, bf16[1024,64]{1,0:T(8,128)(2,1)} %bitcast.12, ...), custom_call_target="tpu_custom_call" | custom-call | tf_op jit(solution)/shard_map/pallas_call | solution.py:434
  52.6 2.0 %shard_map.203 = (bf16[64,2048]{1,0:T(8,128)(2,1)}, bf16[3,64,1024]{2,1,0:T(8,128)(2,1)}, f32[64,1024]{1,0:T(8,128)}) custom-call(bf16[64,2048]{1,0:T(8,128)(2,1)} %get-tuple-element.9.a, bf16[3,64,1024]{2,1,0:T(8,128)(2,1)} %get-tuple-element.10.b, f32[64,1024]{1,0:T(8,128)} %get-tuple-element.11.c), custom_call_target="tpu_custom_call" | custom-call | tf_op jit(solution)/shard_map/pallas_call | solution.py:477
